TPU v7x, 32 devices: a whole 2x2x4 slice. The times are simulated.
32 devices in a mesh: sp: 16 (over z, y, x), tp: 2 (over core).
Axes of the slice: x: 2, y: 2, z: 4, core: 2. Of those that a mesh axis runs over, the one named last changes fastest.
Arguments:
- tokens: bfloat16 [12288, 2048], P(('sp', 'tp')), may hold values from -6 to 6
- input_gain: float32 [2048], replicated, may hold values from 0.1 to 1.9
- branch_value: bfloat16 [2048, 1024], P('sp', 'tp'), may hold values from -0.125 to 0.125
- branch_gate: bfloat16 [2048, 1024], P('sp', 'tp'), may hold values from -0.125 to 0.125
- query_weight: bfloat16 [2048, 1024], P('sp', 'tp'), may hold values from -0.125 to 0.125
- key_weight: bfloat16 [2048, 1024], P('sp', 'tp'), may hold values from -0.125 to 0.125
- value_weight: bfloat16 [2048, 1024], P('sp', 'tp'), may hold values from -0.125 to 0.125
- swish_weight: bfloat16 [2048, 1024], P('sp', 'tp'), may hold values from -0.125 to 0.125
- kernel_taps: float32 [31, 1024], P(None, 'tp'), may hold values from -8 to 8
- channel_gain: float32 [1024], P('tp'), may hold values from 0.1 to 1.9
- decay_logs: float32 [16, 12288], P('tp', 'sp'), may hold values from -1.5 to 0
- start_state: float32 [2, 16, 64, 64], P(None, 'tp')
- head_gain: float32 [1024], P('tp'), may hold values from 0.1 to 1.9
- output_conv: bfloat16 [1024, 2048], P('tp', 'sp'), may hold values from -0.125 to 0.125
- output_heads: bfloat16 [1024, 2048], P('tp', 'sp'), may hold values from -0.125 to 0.125
Outputs:
- mixed: bfloat16 [12288, 2048], P(('sp', 'tp'))
All inputs are finite; a program needn't handle non-finite values.
Results may differ from a plain program's by a relative error of at most 0.018.
Values may be sent and summed in bfloat16 or wider, within the bound.
A program may use at most 64 MiB of HBM per device.

v0:
```python
import functools
import jax
import jax.numpy as jnp
from jax import lax
from jax.experimental import pallas as pl
from jax.experimental.pallas import tpu as pltpu
from jax.sharding import PartitionSpec as P

DC = 1024
HD = 64
BLOCK = 256
SIDE = 2
MESH_ID = pl.DeviceIdType.MESH


class Router:
    def __init__(self, count, rows):
        self.depth = count // (SIDE * SIDE)
        me = lax.axis_index("sp")
        self.x = lax.rem(me, SIDE)
        self.y = lax.rem(me // SIDE, SIDE)
        self.z = me // (SIDE * SIDE)
        tile = 16
        short = rows // (8 * tile) * tile
        long = (rows - 2 * short) // (2 * tile) * tile
        self.routes = (
            ("zxy", 0, rows - 2 * short - long),
            ("zyx", rows - 2 * short - long, long),
            ("xyz", rows - 2 * short, short),
            ("yxz", rows - short, short),
        )
        reach = [(0, None)]
        for d in range(1, self.depth):
            reach += [(-d, self.z - d >= 0), (d, self.z + d < self.depth)]
        self.events = []
        for dz, valid in reach:
            for dy in range(SIDE):
                for dx in range(SIDE):
                    if dz == dy == dx == 0:
                        continue
                    for r, (order, _, _) in enumerate(self.routes):
                        self.events.append((abs(dz) + dy + dx, r, dz, dy, dx, valid))
        self.events.sort(key=lambda e: (e[0], e[1], e[2], e[3], e[4]))

    def index(self, z, y, x):
        return (z * SIDE + y) * SIDE + x

    def source(self, dz, dy, dx):
        y = self.y if dy == 0 else 1 - self.y
        x = self.x if dx == 0 else 1 - self.x
        return self.index(self.z + dz, y, x)

    def neighbours(self):
        z, y, x = self.z, self.y, self.x
        return {
            "x": (self.index(z, y, 1 - x), None),
            "y": (self.index(z, 1 - y, x), None),
            "+": (self.index(z + 1, y, x), z + 1 < self.depth),
            "-": (self.index(z - 1, y, x), z - 1 >= 0),
        }

    def targets(self, r, dz, dy, dx):
        order = self.routes[r][0]
        off = {"z": dz, "y": dy, "x": dx}
        last = max([i for i, d in enumerate(order) if off[d] != 0], default=-1)
        out = []
        if last >= 0 and order[last] == "z":
            out.append("+" if dz < 0 else "-")
        for d in order[last + 1 :]:
            out += ["+", "-"] if d == "z" else [d]
        return out


def when(cond, fn):
    if cond is None:
        fn()
    else:
        pl.when(cond)(fn)


def both(a, b):
    if a is None:
        return b
    if b is None:
        return a
    return jnp.logical_and(a, b)


DIRECTIONS = "xy+-"


def enter(router, partner):
    barrier = pltpu.get_barrier_semaphore()
    near = router.neighbours()
    for idx, valid in near.values():

        def greet(idx=idx):
            pl.semaphore_signal(barrier, inc=1, device_id={"sp": idx}, device_id_type=MESH_ID)

        when(valid, greet)
    extra = 0
    if partner is not None:
        pl.semaphore_signal(barrier, inc=1, device_id={"tp": partner}, device_id_type=MESH_ID)
        extra = 1
    ends = sum(jnp.where(near[d][1], 1, 0) for d in "+-")
    pl.semaphore_wait(barrier, 2 + extra + ends)


class Flow:
    def __init__(self, router, local, gathered, rows, send_sem, recv_sem):
        self.router, self.local, self.gathered, self.rows = router, local, gathered, rows
        self.send_sem, self.recv_sem = send_sem, recv_sem

    def copy(self, g, r, dz, dy, dx, d):
        router = self.router
        _, first, count = router.routes[r]
        s = router.source(dz, dy, dx)
        place = self.gathered.at[g, s, pl.ds(first, count), :]
        src = self.local.at[g, pl.ds(first, count), :] if dz == dy == dx == 0 else place
        idx, valid = router.neighbours()[d]
        k = DIRECTIONS.index(d)
        return (
            pltpu.make_async_remote_copy(
                src_ref=src,
                dst_ref=place,
                send_sem=self.send_sem.at[g, r, k, s],
                recv_sem=self.recv_sem.at[g, r, s],
                device_id={"sp": idx},
                device_id_type=MESH_ID,
            ),
            valid,
        )

    def send(self, g, r, dz, dy, dx, wait=False):
        for d in self.router.targets(r, dz, dy, dx):
            copy, valid = self.copy(g, r, dz, dy, dx, d)
            when(valid, copy.wait_send if wait else copy.start)

    def own(self, g, wait=False):
        for r in range(len(self.router.routes)):
            self.send(g, r, 0, 0, 0, wait)

    def event(self, g, e):
        _, r, dz, dy, dx, cond = e

        def arrived():
            self.copy(g, r, dz, dy, dx, "x")[0].wait_recv()
            self.send(g, r, dz, dy, dx)

        when(cond, arrived)

    def finish(self, g):
        self.own(g, True)
        for e in self.router.events:
            _, r, dz, dy, dx, cond = e
            if self.router.targets(r, dz, dy, dx):
                when(cond, functools.partial(self.send, g, r, dz, dy, dx, True))


def project_kernel(
    count, tokens, gain, local, gated_out, packed_out, last_out,
    gathered, raw, normed, send_sem, recv_sem, local_sem, swap_sem,
):
    groups, rows, width = local.shape
    router = Router(count, rows)
    core = lax.axis_index("tp")
    partner = 1 - core
    own_rows = tokens.shape[0]
    flow = Flow(router, local, gathered, rows, send_sem, recv_sem)
    mine = pl.ds(pl.multiple_of(core * own_rows, own_rows), own_rows)
    me = lax.axis_index("sp")
    enter(router, partner)
    flow.own(0)
    swap = pltpu.make_async_remote_copy(
        src_ref=tokens, dst_ref=raw.at[mine, :], send_sem=swap_sem.at[0], recv_sem=swap_sem.at[1],
        device_id={"tp": partner}, device_id_type=MESH_ID,
    )
    swap.start()
    keep = pltpu.make_async_copy(tokens, raw.at[mine, :], local_sem.at[groups])
    keep.start()
    for g in range(groups):
        pltpu.make_async_copy(local.at[g], gathered.at[g, me], local_sem.at[g]).start()
    for g in range(groups):
        pltpu.make_async_copy(local.at[g], gathered.at[g, me], local_sem.at[g]).wait()
    keep.wait()
    swap.wait()
    n_events = len(router.events)
    half = normed.shape[0] // 2
    tiles = width // 256
    units = 2 * tiles
    norm_rows = normed.shape[0] // units

    def unit(it, u):
        @pl.when(it == 0)
        def _():
            window = pl.ds(u * norm_rows, norm_rows)
            widened = raw[window, :].astype(jnp.float32)
            inverse = lax.rsqrt(jnp.mean(widened * widened, axis=1, keepdims=True) + EPSILON)
            normed[window, :] = (widened * inverse * gain[...]).astype(jnp.bfloat16)

        @pl.when(it > 0)
        def _():
            m, n = u % 2, u // 2
            window = pl.ds(m * half, half)
            weight = gathered[it - 1, :, :, n * 256 : (n + 1) * 256].reshape(count * rows, 256)
            product = jnp.dot(normed[window, :], weight, preferred_element_type=jnp.float32)

            @pl.when(it == 1)
            def _():
                gated_out[window, n * 128 : (n + 1) * 128] = (
                    product[:, :128] * jax.nn.sigmoid(product[:, 128:])
                ).astype(jnp.bfloat16)

            @pl.when(it > 1)
            def _():
                column = pl.multiple_of((it - 2) * width + n * 256, 256)
                packed_out[window, pl.ds(column, 256)] = product.astype(jnp.bfloat16)

    def step(it, _):
        @pl.when(it < groups - 1)
        def _():
            flow.own(it + 1)

        done = 0
        for i, e in enumerate(router.events):
            flow.event(it, e)
            while done < units and (i + 1) * units >= (done + 1) * n_events:
                unit(it, done)
                done += 1
        return 0

    lax.fori_loop(0, groups, step, 0)
    last = gathered.at[groups - 1]

    def place(s, _):
        for j in range(width // rows):
            pltpu.make_async_copy(
                last.at[s, :, pl.ds(j * rows, rows)],
                last_out.at[pl.ds(j * rows, rows), pl.ds(pl.multiple_of(s * rows, rows), rows)],
                local_sem.at[0],
            ).start()
        return 0

    lax.fori_loop(0, count, place, 0)

    def drain(g, _):
        flow.finish(g)
        return 0

    lax.fori_loop(0, groups, drain, 0)
    pltpu.make_async_copy(last, last, local_sem.at[0]).wait()


def project(count, tokens, gain, local):
    groups, rows, width = local.shape
    total = tokens.shape[0] * 2
    model = tokens.shape[1]
    vmem = pl.BlockSpec(memory_space=pltpu.VMEM)
    return pl.pallas_call(
        functools.partial(project_kernel, count),
        out_shape=(
            jax.ShapeDtypeStruct((total, width // 2), jnp.bfloat16),
            jax.ShapeDtypeStruct((total, (groups - 2) * width), jnp.bfloat16),
            jax.ShapeDtypeStruct((width, count * rows), jnp.bfloat16),
        ),
        in_specs=[vmem] * 3,
        out_specs=(vmem, vmem, pl.BlockSpec(memory_space=pl.ANY)),
        scratch_shapes=[
            pltpu.VMEM((groups, count, rows, width), jnp.bfloat16),
            pltpu.VMEM((total, model), jnp.bfloat16),
            pltpu.VMEM((total, model), jnp.bfloat16),
            pltpu.SemaphoreType.DMA((groups, 4, 4, count)),
            pltpu.SemaphoreType.DMA((groups, 4, count)),
            pltpu.SemaphoreType.DMA((groups + 1,)),
            pltpu.SemaphoreType.DMA((2,)),
        ],
        compiler_params=pltpu.CompilerParams(
            collective_id=0, has_side_effects=True, vmem_limit_bytes=60 * 1024 * 1024
        ),
        name="project",
    )(tokens, gain.reshape(1, -1), local)


def gather_kernel(count, local, gathered, send_sem, recv_sem, local_sem):
    _, rows, _ = local.shape
    router = Router(count, rows)
    flow = Flow(router, local, gathered, rows, send_sem, recv_sem)
    enter(router, None)
    flow.own(0)
    keep = pltpu.make_async_copy(local.at[0], gathered.at[0, lax.axis_index("sp")], local_sem.at[0])
    keep.start()
    for e in router.events:
        flow.event(0, e)
    keep.wait()
    flow.finish(0)


def gather_small(count, local):
    rows, width = local.shape
    vmem = pl.BlockSpec(memory_space=pltpu.VMEM)
    return pl.pallas_call(
        functools.partial(gather_kernel, count),
        out_shape=jax.ShapeDtypeStruct((1, count, rows, width), local.dtype),
        in_specs=[vmem],
        out_specs=vmem,
        scratch_shapes=[
            pltpu.SemaphoreType.DMA((1, 4, 4, count)),
            pltpu.SemaphoreType.DMA((1, 4, count)),
            pltpu.SemaphoreType.DMA((1,)),
        ],
        compiler_params=pltpu.CompilerParams(collective_id=1, has_side_effects=True),
        name="gather_states",
    )(local[None])[0]


EPSILON = 1e-06
HIGHEST = lax.Precision.HIGHEST


def with_halo(x, sides, width):
    for axis, dim in sides:
        count, length = (lax.axis_size(axis), x.shape[dim])
        up = [(i, (i + 1) % count) for i in range(count - 1)]
        down = [(j, i) for i, j in up]
        last = lax.slice_in_dim(x, length - width, length, axis=dim)
        first = lax.slice_in_dim(x, 0, width, axis=dim)
        before = lax.ppermute(last, axis, up)
        after = lax.ppermute(first, axis, down)
        x = jnp.concatenate([before, x, after], axis=dim)
    return x


def prefix(x, axis, join, neutral, backward):
    count = lax.axis_size(axis)
    place = lax.axis_index(axis)
    ahead = count - 1 - place if backward else place
    gathered = jax.tree.map(
        lambda a, kind: lax.all_gather(a.astype(kind), axis), x, (jnp.bfloat16, jnp.bfloat16)
    )
    state = jax.tree.map(lambda a, e: jnp.zeros_like(a) + jnp.asarray(e, a.dtype), x, neutral)

    def one(step, state):
        source = count - 1 - step if backward else step
        return join(
            state,
            jax.tree.map(
                lambda a, own: lax.dynamic_index_in_dim(a, source, 0, False).astype(own.dtype),
                gathered,
                x,
            ),
        )

    return lax.fori_loop(0, ahead, one, state)


def block_states(scaled_keys, values_block, running):
    closing = running[:, :, -1:]
    totals = jnp.exp(closing[:, :, 0])
    toward_end = jnp.exp(closing - running).transpose(0, 2, 1)[:, :, :, None]
    from_start = jnp.exp(running).transpose(0, 2, 1)[:, :, :, None]
    forward = jnp.einsum(
        "nshd,nshe->nhde", scaled_keys * toward_end, values_block, precision=HIGHEST
    )
    backward = jnp.einsum(
        "nshd,nshe->nhde", scaled_keys * from_start, values_block, precision=HIGHEST
    )
    return (totals, forward, backward)


def block_outputs(queries, scaled_keys, values_block, running, forward_in, backward_in):
    length = queries.shape[1]
    scores = jnp.einsum("nthd,nshd->nhts", queries, scaled_keys, precision=HIGHEST)
    distance = jnp.abs(running[:, :, :, None] - running[:, :, None, :])
    weights = jnp.exp(-distance) + jnp.eye(length, dtype=jnp.float32)
    within = jnp.einsum("nhts,nshe->nthe", scores * weights, values_block, precision=HIGHEST)
    from_start = jnp.exp(running).transpose(0, 2, 1)[:, :, :, None]
    toward_end = jnp.exp(running[:, :, -1:] - running).transpose(0, 2, 1)[:, :, :, None]
    earlier = jnp.einsum("nthd,nhde->nthe", queries, forward_in, precision=HIGHEST)
    after_part = jnp.einsum("nthd,nhde->nthe", queries, backward_in, precision=HIGHEST)
    return within + from_start * earlier + toward_end * after_part


def head_output(retained, gates_in, head_gain):
    row_count = retained.shape[0]
    centred = retained - jnp.mean(retained, axis=2, keepdims=True)
    scaled = centred * lax.rsqrt(jnp.mean(centred * centred, axis=2, keepdims=True) + EPSILON)
    flattened = scaled.reshape(row_count, -1) * head_gain[None, :]
    return (flattened * jax.nn.silu(gates_in.astype(jnp.float32))).astype(jnp.bfloat16)


def normalize(token_block, input_gain):
    widened = token_block.astype(jnp.float32)
    inverse = lax.rsqrt(jnp.mean(widened * widened, axis=1, keepdims=True) + EPSILON)
    return (widened * inverse * input_gain[None, :]).astype(jnp.bfloat16)


def input_mix(products):
    gated_rows = (products[0] * jax.nn.sigmoid(products[1])).astype(jnp.bfloat16)
    others = [member.astype(jnp.bfloat16) for member in products[2:]]
    return jnp.concatenate([gated_rows] + others, axis=1)


def combine_branches(earlier, latter):
    return (earlier[0] * latter[0], latter[0][:, None, None] * earlier[1] + latter[1])


def states_kernel(packed, end_scale, start_scale, forward, backward):
    rows, wide = packed.shape
    width = wide // 4
    pair = 2 * HD
    first = lax.broadcasted_iota(jnp.int32, (rows, pair), 1) < HD
    for h in range(0, width // HD, 2):
        at = h * HD
        keys = packed[:, width + at : width + at + pair].astype(jnp.float32) * HD ** (-0.5)
        values = packed[:, 2 * width + at : 2 * width + at + pair]
        for scale, out in ((end_scale, forward), (start_scale, backward)):
            factor = jnp.where(first, scale[:, h : h + 1], scale[:, h + 1 : h + 2])
            state = lax.dot_general(
                (keys * factor).astype(jnp.bfloat16), values, (((0,), (0,)), ((), ())),
                preferred_element_type=jnp.float32,
            )
            out[0, h] = state[:HD, :HD]
            out[0, h + 1] = state[HD:, HD:]


def fast_states(packed, running):
    blocks, heads, length = running.shape
    closing = running[:, :, -1:]
    end_scale = jnp.exp(closing - running).transpose(0, 2, 1).reshape(-1, heads)
    start_scale = jnp.exp(running).transpose(0, 2, 1).reshape(-1, heads)
    rows = pl.BlockSpec((length, packed.shape[1]), lambda n: (n, 0))
    scale = pl.BlockSpec((length, heads), lambda n: (n, 0))
    state = pl.BlockSpec((1, heads, HD, HD), lambda n: (n, 0, 0, 0))
    shape = jax.ShapeDtypeStruct((blocks, heads, HD, HD), jnp.float32)
    forward, backward = pl.pallas_call(
        states_kernel, grid=(blocks,), in_specs=[rows, scale, scale],
        out_specs=(state, state), out_shape=(shape, shape), name="block_states",
    )(packed, end_scale, start_scale)
    return jnp.exp(closing[:, :, 0]), forward, backward


def retain_kernel(packed, column, row, forward_in, backward_in, gain, out):
    rows, wide = packed.shape
    width = wide // 4
    pair = 2 * HD
    t = lax.broadcasted_iota(jnp.int32, (rows, rows), 0)
    s = lax.broadcasted_iota(jnp.int32, (rows, rows), 1)
    same = jnp.where(t == s, 1.0, 0.0)
    for h in range(0, width // HD, 2):
        at = h * HD
        q, k, v, g = (packed[:, i * width + at : i * width + at + pair] for i in range(4))
        done = []
        for i in range(2):
            lanes = slice(i * HD, (i + 1) * HD)
            head = h + i
            scores = lax.dot_general(
                q[:, lanes], k[:, lanes], (((1,), (1,)), ((), ())),
                preferred_element_type=jnp.float32,
            ) * HD ** (-0.5)
            down = column[:, head : head + 1]
            along = row[0, head : head + 1, :]
            weights = jnp.exp(-jnp.abs(down - along)) + same
            within = jnp.dot(
                (scores * weights).astype(jnp.bfloat16), v[:, lanes],
                preferred_element_type=jnp.float32,
            )
            entering = [
                jnp.dot(q[:, lanes], state[0, head].astype(jnp.bfloat16),
                        preferred_element_type=jnp.float32)
                for state in (forward_in, backward_in)
            ]
            closing = column[rows - 1 : rows, head : head + 1]
            kept = within + jnp.exp(down) * entering[0] + jnp.exp(closing - down) * entering[1]
            centred = kept - jnp.mean(kept, axis=1, keepdims=True)
            done.append(
                centred * lax.rsqrt(jnp.mean(centred * centred, axis=1, keepdims=True) + EPSILON)
            )
        both_heads = jnp.concatenate(done, axis=1) * gain[:, at : at + pair]
        out[:, at : at + pair] = (both_heads * jax.nn.silu(g.astype(jnp.float32))).astype(
            jnp.bfloat16
        )


def fast_retention(packed, running, forward_in, backward_in, head_gain):
    blocks, heads, length = running.shape
    column = running.transpose(0, 2, 1).reshape(-1, heads)
    width = heads * HD
    state = pl.BlockSpec((1, heads, HD, HD), lambda n: (n, 0, 0, 0))
    return pl.pallas_call(
        retain_kernel, grid=(blocks,),
        in_specs=[
            pl.BlockSpec((length, packed.shape[1]), lambda n: (n, 0)),
            pl.BlockSpec((length, heads), lambda n: (n, 0)),
            pl.BlockSpec((1, heads, length), lambda n: (n, 0, 0)),
            state, state,
            pl.BlockSpec((1, width), lambda n: (0, 0)),
        ],
        out_specs=pl.BlockSpec((length, width), lambda n: (n, 0)),
        out_shape=jax.ShapeDtypeStruct((packed.shape[0], width), jnp.bfloat16),
        name="retain",
    )(packed, column, running, forward_in, backward_in, head_gain.reshape(1, -1))


def fits(tokens, weight, output):
    return (
        lax.axis_size("tp") == 2
        and lax.axis_size("sp") % (SIDE * SIDE) == 0
        and weight.shape == (128, 512)
        and output.shape == (512, 128)
        and tokens.shape[0] % 128 == 0
    )


def general_projections(tokens, input_gain, projections):
    group_rows = lax.all_gather(tokens, "tp", axis=0, tiled=True)
    normed = normalize(group_rows, input_gain)
    portions = (
        lax.all_gather(projections[0], "sp", axis=0, tiled=True),
        lax.all_gather(projections[1], "sp", axis=0, tiled=True),
        lax.all_gather(projections[2], "sp", axis=0, tiled=True),
        lax.all_gather(projections[3], "sp", axis=0, tiled=True),
        lax.all_gather(projections[4], "sp", axis=0, tiled=True),
        lax.all_gather(projections[5], "sp", axis=0, tiled=True),
    )
    return input_mix(
        tuple(
            (jnp.dot(normed, portion, preferred_element_type=jnp.float32) for portion in portions)
        )
    )


def fast_prefix(running, forward, backward):
    count = lax.axis_size("sp")
    me = lax.axis_index("sp")
    heads, width = forward.shape[0], forward.shape[1]
    logs = jnp.sum(running[:, :, -1], axis=0)
    coarse = lax.reduce_precision(logs, 8, 7)
    pair = jnp.concatenate([coarse, logs - coarse]).astype(jnp.bfloat16)
    extra = jnp.zeros((16, 128), jnp.bfloat16).at[0, : 2 * heads].set(pair)
    both_states = jnp.stack([forward, backward]).astype(jnp.bfloat16).reshape(-1, 128)
    cut = both_states.shape[0]
    arrived = gather_small(count, jnp.concatenate([both_states, extra], axis=0))
    states = arrived[:, :cut].reshape(count, 2, heads, width, width)
    pair = arrived[:, cut, : 2 * heads].astype(jnp.float32)
    logs = pair[:, :heads] + pair[:, heads:]
    place = jnp.arange(count)
    inner = place[None, :]
    outer = place[:, None]
    left = (inner > outer) & (inner < me)
    right = (inner < outer) & (inner > me)
    left_log = jnp.sum(jnp.where(left[:, :, None], logs[None], 0.0), axis=1)
    right_log = jnp.sum(jnp.where(right[:, :, None], logs[None], 0.0), axis=1)
    left_scale = jnp.where((place < me)[:, None], jnp.exp(left_log), 0.0)
    right_scale = jnp.where((place > me)[:, None], jnp.exp(right_log), 0.0)
    wide = states.astype(jnp.float32)
    enter_left = jnp.sum(left_scale[:, :, None, None] * wide[:, 0], axis=0)
    enter_right = jnp.sum(right_scale[:, :, None, None] * wide[:, 1], axis=0)
    total_left = jnp.exp(jnp.sum(jnp.where((place < me)[:, None], logs, 0.0), axis=0))
    total_right = jnp.exp(jnp.sum(jnp.where((place > me)[:, None], logs, 0.0), axis=0))
    return (total_left, enter_left), (total_right, enter_right)


def body(
    tokens,
    input_gain,
    branch_value,
    branch_gate,
    query_weight,
    key_weight,
    value_weight,
    swish_weight,
    kernel_taps,
    channel_gain,
    decay_logs,
    start_state,
    head_gain,
    output_conv,
    output_heads,
):
    value_width = branch_value.shape[1]
    head_width = query_weight.shape[1]
    fast = fits(tokens, branch_value, output_conv)
    if fast:
        rows = branch_value.shape[0]

        def mixed_columns(a, b):
            return jnp.stack(
                [a.reshape(rows, -1, 128), b.reshape(rows, -1, 128)], axis=2
            ).reshape(rows, -1)

        outputs = jnp.concatenate([output_conv, output_heads], axis=0)
        cut = outputs.shape[1]
        local = jnp.stack(
            [
                mixed_columns(branch_value, branch_gate),
                jnp.concatenate([query_weight, key_weight], axis=1),
                jnp.concatenate([value_weight, swish_weight], axis=1),
                outputs.reshape(-1, cut, cut).transpose(1, 0, 2).reshape(cut, -1),
            ]
        )
        gated_rows, packed, out_weights = project(lax.axis_size("sp"), tokens, input_gain, local)
    else:
        packed = general_projections(
            tokens, input_gain,
            (branch_value, branch_gate, query_weight, key_weight, value_weight, swish_weight),
        )
        gated_rows = packed[:, :value_width]
        packed = packed[:, value_width:]
    row_count = packed.shape[0]
    queries_in = packed[:, :head_width]
    keys_in = packed[:, head_width : 2 * head_width]
    values_in = packed[:, 2 * head_width : 3 * head_width]
    gates_in = packed[:, 3 * head_width :]
    half_width = kernel_taps.shape[0] // 2
    padded = with_halo(gated_rows, (("sp", 0),), half_width).astype(jnp.float32)
    convolved = jnp.zeros((row_count, value_width), jnp.float32)
    for offset in range(kernel_taps.shape[0]):
        convolved = convolved + kernel_taps[offset][None, :] * padded[offset : offset + row_count]
    moments = lax.psum((jnp.sum(convolved, axis=1), jnp.sum(convolved * convolved, axis=1)), "tp")
    average = (moments[0] / DC)[:, None]
    squares = (moments[1] / DC)[:, None]
    normalized = (convolved - average) * lax.rsqrt(squares - average * average + EPSILON)
    branch_out = jax.nn.silu(normalized * channel_gain[None, :]).astype(jnp.bfloat16)
    local_heads = head_width // HD
    blocks = row_count // BLOCK

    def split_heads(matrix):
        return matrix.astype(jnp.float32).reshape(blocks, BLOCK, local_heads, HD)

    query_blocks = split_heads(queries_in)
    key_blocks = split_heads(keys_in) * HD ** (-0.5)
    value_blocks = split_heads(values_in)
    running = jnp.cumsum(decay_logs.reshape(local_heads, blocks, BLOCK).transpose(1, 0, 2), axis=2)
    if fast:
        totals, forward, backward = fast_states(packed, running)
    else:
        totals, forward, backward = block_states(key_blocks, value_blocks, running)
    forward_part = []
    forward_scale = []
    carried = jnp.zeros_like(forward[0])
    factor = jnp.ones_like(totals[0])
    for block_index in range(blocks):
        forward_part.append(carried)
        forward_scale.append(factor)
        carried = totals[block_index][:, None, None] * carried + forward[block_index]
        factor = factor * totals[block_index]
    device_forward = carried
    device_total = factor
    backward_part = [None] * blocks
    reverse_direction_scale = [None] * blocks
    carried = jnp.zeros_like(backward[0])
    factor = jnp.ones_like(totals[0])
    for block_index in reversed(range(blocks)):
        backward_part[block_index] = carried
        reverse_direction_scale[block_index] = factor
        carried = totals[block_index][:, None, None] * carried + backward[block_index]
        factor = factor * totals[block_index]
    identity = (jnp.ones_like(device_total), jnp.zeros_like(device_forward))
    if fast:
        before, after = fast_prefix(running, device_forward, carried)
    else:
        before = prefix((device_total, device_forward), "sp", combine_branches, identity, False)
        after = prefix((device_total, carried), "sp", combine_branches, identity, True)
    enter_forward = before[1] + before[0][:, None, None] * start_state[0]
    enter_backward = after[1] + after[0][:, None, None] * start_state[1]
    forward_in = jnp.stack(
        [
            forward_scale[block_index][:, None, None] * enter_forward + forward_part[block_index]
            for block_index in range(blocks)
        ]
    )
    backward_in = jnp.stack(
        [
            reverse_direction_scale[block_index][:, None, None] * enter_backward
            + backward_part[block_index]
            for block_index in range(blocks)
        ]
    )
    if fast:
        heads_out = fast_retention(packed, running, forward_in, backward_in, head_gain)
    else:
        retained = block_outputs(
            query_blocks, key_blocks, value_blocks, running, forward_in, backward_in
        )
        heads_out = head_output(retained.reshape(row_count, local_heads, HD), gates_in, head_gain)
    if fast:
        partial_sum = jnp.dot(
            jnp.concatenate([branch_out, heads_out], axis=1),
            out_weights,
            preferred_element_type=jnp.float32,
        ).astype(jnp.bfloat16)
        halves = partial_sum.reshape(2, row_count // 2, -1)
        core = lax.axis_index("tp")
        mine = lax.dynamic_index_in_dim(halves, core, 0, False)
        other = lax.dynamic_index_in_dim(halves, 1 - core, 0, False)
        received = lax.ppermute(other, "tp", [(0, 1), (1, 0)])
        return (mine.astype(jnp.float32) + received.astype(jnp.float32)).astype(jnp.bfloat16)
    out_columns = (
        lax.all_gather(output_conv, "sp", axis=1, tiled=True),
        lax.all_gather(output_heads, "sp", axis=1, tiled=True),
    )
    combined = jnp.dot(branch_out, out_columns[0], preferred_element_type=jnp.float32)
    return lax.psum_scatter(
        (combined + jnp.dot(heads_out, out_columns[1], preferred_element_type=jnp.float32)).astype(
            jnp.bfloat16
        ),
        "tp",
        scatter_dimension=0,
        tiled=True,
    )


def solution(mesh):
    in_specs = (
        P(("sp", "tp"), None),
        P(),
        P("sp", "tp"),
        P("sp", "tp"),
        P("sp", "tp"),
        P("sp", "tp"),
        P("sp", "tp"),
        P("sp", "tp"),
        P(None, "tp"),
        P("tp"),
        P("tp", "sp"),
        P(None, "tp", None, None),
        P("tp"),
        P("tp", "sp"),
        P("tp", "sp"),
    )
    out_specs = P(("sp", "tp"), None)
    return jax.shard_map(body, mesh=mesh, in_specs=in_specs, out_specs=out_specs, check_vma=False)
```

profile of v0, /device:TPU:0, one launch (start us, length us, event | category | flops | bytes accessed | tf_op | source)
XLA Modules:
  0.0 260.1 jit_solution(16016160133612563271)
XLA Ops:
  0.0 1.0 pad_maximum_fusion.4
  1.6 0.6 pad_maximum_fusion.3
  2.4 1.1 pad_maximum_fusion.local
  3.6 147.7 %project.1 = (bf16[768,512]{1,0:T(8,128)(2,1)}, bf16[768,2048]{1,0:T(8,128)(2,1)}, bf16[1024,2048]{1,0:T(8,128)(2,1)}) custom-call(bf16[384,2048]{1,0:T(8,128)(2,1)} %tokens.1, f32[1,2048]{1,0:T(1,128)} %bitcast.125, bf16[4,128,1024]{2,1,0:T(8,128)(2,1)} %pad_maximum_fusion.local), custom_call_target="tpu_custom_call" | custom-call | tf_op jit(solution)/shard_map/project/pallas_call | solution.py:259
  151.3 0.7 fusion.54
  152.1 1.3 collective-permute-start.1
  153.3 4.9 %collective-permute-start = (bf16[15,512]{1,0:T(8,128)(2,1)S(1)}, bf16[15,512]{1,0:T(8,128)(2,1)S(1)}, u32[]{:S(2)}, u32[]{:S(2)}) collective-permute-start(bf16[15,512]{1,0:T(8,128)(2,1)S(1)} %get-tuple-element.47), channel_id=1, source_target_pairs={{0,2},{2,4},{4,6},{6,8},{8,10},{10,12},{12,14},{14,16},{16,18},{18... | collective-permute-start | bytes 46088 | tf_op jit(solution)/shard_map/ppermute | solution.py:327
  158.2 1.7 reduce-window.6
  160.3 0.2 slice_reduce_fusion.2
  160.6 0.9 copy.28.end_scale
  161.5 0.9 copy.29.start_scale
  162.5 9.9 %block_states.1 = (f32[3,8,64,64]{3,2,1,0:T(8,128)}, f32[3,8,64,64]{3,2,1,0:T(8,128)}) custom-call(bf16[768,2048]{1,0:T(8,128)(2,1)} %get-tuple-element.23.packed, f32[768,8]{1,0:T(8,128)} %copy.28.end_scale, f32[768,8]{1,0:T(8,128)} %copy.29.start_scale), custom_call_target="tpu_custom_call" | custom-call | tf_op jit(solution)/shard_map/block_states/pallas_call | solution.py:435
  172.3 1.5 add_convert_fusion.1
  174.1 0.7 maximum_bitcast_fusion.2.local
  174.8 26.1 %gather_states.1 = bf16[1,16,528,128]{3,2,1,0:T(8,128)(2,1)} custom-call(bf16[1,528,128]{2,1,0:T(8,128)(2,1)} %maximum_bitcast_fusion.2.local), custom_call_target="tpu_custom_call" | custom-call | tf_op jit(solution)/shard_map/gather_states/pallas_call | solution.py:301
  201.0 0.8 slice_convert_fusion.1
  201.7 4.0 %slice_convert_fusion = f32[16,512,128]{2,1,0:T(8,128)} fusion(bf16[16,528,128]{2,1,0:T(8,128)(2,1)} %bitcast.113), kind=kLoop, calls=%fused_computation.9 | loop fusion | flops 1048576 | bytes 6291456 | tf_op jit(solution)/shard_map/convert_element_type | solution.py:555
  205.9 7.0 %reshape.246 = f32[16,2,8,64,64]{4,3,2,1,0:T(8,128)} reshape(f32[16,512,128]{2,1,0:T(8,128)} %slice_convert_fusion) | data formatting | bytes 8388608 | tf_op jit(solution)/shard_map/convert_element_type | solution.py:555
  213.3 4.1 %fusion.1 = (f32[8,64,64]{2,1,0:T(8,128)S(1)}, f32[8,64,64]{2,1,0:T(8,128)S(1)}) fusion(f32[16,2,8,64,64]{4,3,2,1,0:T(8,128)} %reshape.246, f32[16,8]{1,0:T(8,128)S(1)} %exponential_select_fusion, f32[16,8]{1,0:T(8,128)S(1)} %exponential_select_fusion.1), kind=kLoop, calls=%fused_computation.2 | loop fusion | flops 2031616 | bytes 4457472 | tf_op jit(solution)/shard_map/reduce_sum | solution.py:557
  217.4 0.2 multiply_add_fusion.1
  217.9 1.0 pad_maximum_fusion.1.forward_in
  218.8 0.9 pad_maximum_fusion.2.backward_in
  219.8 0.9 copy.31.column
  220.7 15.3 %retain.1 = bf16[768,512]{1,0:T(8,128)(2,1)} custom-call(bf16[768,2048]{1,0:T(8,128)(2,1)} %get-tuple-element.23.packed, f32[768,8]{1,0:T(8,128)} %copy.31.column, f32[3,8,256]{2,1,0:T(8,128)} %bitcast.120, f32[3,8,64,64]{3,2,1,0:T(8,128)} %pad_maximum_fusion.1.forward_in, f32[3,8,64,64]{3,2,1,0:T(8,128)} %pad_maximum_fusion.2.backward_in, f32[1,512]{1,0:T(1,128)} %bitcast.157), custom_call_target="tpu_custom_call" | custom-call | tf_op jit(solution)/shard_map/retain/pallas_call | solution.py:489
  236.0 0.2 maximum_convert_fusion
  236.3 6.8 %fusion.52 = (f32[768]{0:T(1024)S(1)}, f32[768]{0:T(1024)S(1)}, f32[768,512]{1,0:T(8,128)S(1)}) fusion(f32[798,512]{1,0:T(8,128)S(1)} %maximum_convert_fusion, f32[512]{0:T(512)S(1)} %bitcast.136, f32[512]{0:T(512)S(1)} %bitcast.137, f32[512]{0:T(512)S(1)} %bitcast.139, f32[512]{0:T(512)S(1)} %bitcast.140, f32[512]{0:T(512)S(1)} %bitcast.141, ...), kind=kLoop, calls=%fused_computation.143 | loop fusion | flops 25164288 | bytes 50401280 | tf_op jit(solution)/shard_map/reduce_sum | solution.py:619
  243.1 2.5 all-reduce.1
  245.6 0.5 multiply_convert_fusion
  246.1 5.8 %convolution_convert_fusion = bf16[768,2048]{1,0:T(8,128)(2,1)S(1)} fusion(bf16[1024,2048]{1,0:T(8,128)(2,1)} %get-tuple-element.26, bf16[768,512]{1,0:T(8,128)(2,1)} %retain.1, bf16[768,512]{1,0:T(8,128)(2,1)S(1)} %multiply_convert_fusion), kind=kOutput, calls=%fused_computation.6 | convolution fusion | flops 3225944064 | bytes 8912896 | tf_op jit(solution)/shard_map/dot_general | solution.py:687
  252.0 1.3 dynamic-slice_bitcast_fusion
  253.4 3.6 %collective-permute-done.2 = bf16[384,2048]{1,0:T(8,128)(2,1)} collective-permute-done((bf16[384,2048]{1,0:T(8,128)(2,1)}, bf16[384,2048]{1,0:T(8,128)(2,1)}, u32[]{:S(2)}, u32[]{:S(2)}) %collective-permute-start.2) | collective-permute-done | bytes 1572896 | tf_op jit(solution)/shard_map/ppermute | solution.py:696
  257.0 3.2 %fusion.4 = bf16[384,2048]{1,0:T(8,128)(2,1)} fusion(bf16[384,2048]{1,0:T(8,128)(2,1)} %collective-permute-done.2, bf16[2,384,2048]{2,1,0:T(8,128)(2,1)S(1)} %bitcast.115, s32[]{:T(128)S(6)} %select_n.41), kind=kLoop, calls=%fused_computation.8 | loop fusion | flops 3145728 | bytes 4718596 | tf_op jit(solution)/shard_map/convert_element_type | solution.py:697
  (64 shorter events, 2.3 us)
Async XLA Ops:
  0.0 1.4 copy-start.5
  0.0 1.5 copy-start.6
  1.0 1.3 copy-start.7
  1.0 1.3 copy-start.8
  1.1 1.3 copy-start.9
  1.1 1.3 copy-start.10
  3.6 154.7 %copy-start.12 = (f32[8,768]{1,0:T(8,128)S(1)}, f32[8,768]{1,0:T(8,128)}, u32[]{:S(2)}) copy-start(f32[8,768]{1,0:T(8,128)} %param.27) | copy-start | bytes 73732
  152.1 84.0 %collective-permute-start.1 = (bf16[15,512]{1,0:T(8,128)(2,1)S(1)}, bf16[15,512]{1,0:T(8,128)(2,1)S(1)}, u32[]{:S(2)}, u32[]{:S(2)}) collective-permute-start(bf16[15,512]{1,0:T(8,128)(2,1)S(1)} %get-tuple-element.48), channel_id=1, source_target_pairs={{2,0},{4,2},{6,4},{8,6},{10,8},{12,10},{14,12},{16,14},{18,16},{20... | collective-permute-start | bytes 46088 | tf_op jit(solution)/shard_map/ppermute | solution.py:328
  153.3 82.7 %collective-permute-start = (bf16[15,512]{1,0:T(8,128)(2,1)S(1)}, bf16[15,512]{1,0:T(8,128)(2,1)S(1)}, u32[]{:S(2)}, u32[]{:S(2)}) collective-permute-start(bf16[15,512]{1,0:T(8,128)(2,1)S(1)} %get-tuple-element.47), channel_id=1, source_target_pairs={{0,2},{2,4},{4,6},{6,8},{8,10},{10,12},{12,14},{14,16},{16,18},{18... | collective-permute-start | bytes 46088 | tf_op jit(solution)/shard_map/ppermute | solution.py:327
  160.2 59.6 %copy-start.4 = (f32[3,8,2,128]{3,1,2,0:T(8,128)}, f32[3,8,2,128]{3,1,2,0:T(8,128)S(1)}, u32[]{:S(2)}) copy-start(f32[3,8,2,128]{3,1,2,0:T(8,128)S(1)} %get-tuple-element.46) | copy-start | bytes 73732
  201.7 4.0 %copy-start.11 = (f32[31,512]{1,0:T(8,128)S(1)}, f32[31,512]{1,0:T(8,128)}, u32[]{:S(2)}) copy-start(f32[31,512]{1,0:T(8,128)} %param.25) | copy-start | bytes 190468
  213.2 4.2 %copy-start = (f32[3,8,64,64]{3,2,1,0:T(8,128)S(1)}, f32[3,8,64,64]{3,2,1,0:T(8,128)}, u32[]{:S(2)}) copy-start(f32[3,8,64,64]{3,2,1,0:T(8,128)} %get-tuple-element.25) | copy-start | bytes 1179652
  213.3 4.2 %copy-start.1 = (f32[3,8,64,64]{3,2,1,0:T(8,128)S(1)}, f32[3,8,64,64]{3,2,1,0:T(8,128)}, u32[]{:S(2)}) copy-start(f32[3,8,64,64]{3,2,1,0:T(8,128)} %get-tuple-element.24) | copy-start | bytes 1179652
  213.3 4.2 %copy-start.3 = (f32[2,8,64,64]{3,2,1,0:T(8,128)S(1)}, f32[2,8,64,64]{3,2,1,0:T(8,128)}, u32[]{:S(2)}) copy-start(f32[2,8,64,64]{3,2,1,0:T(8,128)} %param.28) | copy-start | bytes 786436
  220.7 15.3 %copy-start.2 = (bf16[768,512]{1,0:T(8,128)(2,1)S(1)}, bf16[768,512]{1,0:T(8,128)(2,1)}, u32[]{:S(2)}) copy-start(bf16[768,512]{1,0:T(8,128)(2,1)} %get-tuple-element.22) | copy-start | bytes 2359300
  236.3 9.3 %copy-start.13 = (f32[512]{0:T(512)S(1)}, f32[512]{0:T(512)}, u32[]{:S(2)}) copy-start(f32[512]{0:T(512)} %param.26) | copy-start | bytes 6148
  253.2 3.8 %collective-permute-start.2 = (bf16[384,2048]{1,0:T(8,128)(2,1)}, bf16[384,2048]{1,0:T(8,128)(2,1)}, u32[]{:S(2)}, u32[]{:S(2)}) collective-permute-start(bf16[384,2048]{1,0:T(8,128)(2,1)} %dynamic-slice_bitcast_fusion), channel_id=1, source_target_pairs={{0,1},{1,0},{2,3},{3,2},{4,5},{5,4},{6,7},{7,6},{8,9},{9,8},{10,11... | collective-permute-start | bytes 4718600 | tf_op jit(solution)/shard_map/ppermute | solution.py:696
where the time goes:
time: 261 us; the launch traced here: 260 us
  Pallas kernels  199 us (76%)
  other arithmetic  29.5 us (11%)
  local copies, waits for them, and re-layouts  12.9 us (5%)
  starting transfers between devices  6.32 us (2%)
  matrix products  5.85 us (2%)
  waiting for transfers between devices  3.59 us (1%)
    pallas_call x1, Pallas kernels, project(): pl.pallas_call(functools.partial(project_kernel, count), out_shape=(jax.S...  148 us
    pallas_call x1, Pallas kernels, gather_small(): pl.pallas_call(functools.partial(gather_kernel, count), out_shape=jax.Sha...  26.1 us
    pallas_call x1, Pallas kernels, fast_retention(): pl.pallas_call(retain_kernel, grid=(blocks,), in_specs=[pl.BlockSpec((len...  15.3 us
    pallas_call x1, Pallas kernels, fast_states(): pl.pallas_call(states_kernel, grid=(blocks,), in_specs=[rows, scale, scal...  9.85 us
    convert_element_type x1, local copies, waits for them, and re-layouts, fast_prefix(): wide = states.astype(jnp.float32)  6.96 us
    reduce_sum x1, other arithmetic, body(): jnp.sum(convolved, axis=1)  6.77 us
    dot_general x1, matrix products, body(): jnp.dot(jnp.concatenate([branch_out, heads_out], axis=1), out_weights, pr...  5.85 us
  transfers between devices with their start and end apart: 3, of which 1 were waited for; matrix products, arithmetic and copies ran while one was open for 10% of the time, Pallas kernels for 20%

commit v1 on v0

--- a/solution.py
+++ b/solution.py
@@ -540,7 +540,6 @@
     both_states = jnp.stack([forward, backward]).astype(jnp.bfloat16).reshape(-1, 128)
     cut = both_states.shape[0]
     arrived = gather_small(count, jnp.concatenate([both_states, extra], axis=0))
-    states = arrived[:, :cut].reshape(count, 2, heads, width, width)
     pair = arrived[:, cut, : 2 * heads].astype(jnp.float32)
     logs = pair[:, :heads] + pair[:, heads:]
     place = jnp.arange(count)
@@ -552,9 +551,10 @@
     right_log = jnp.sum(jnp.where(right[:, :, None], logs[None], 0.0), axis=1)
     left_scale = jnp.where((place < me)[:, None], jnp.exp(left_log), 0.0)
     right_scale = jnp.where((place > me)[:, None], jnp.exp(right_log), 0.0)
-    wide = states.astype(jnp.float32)
-    enter_left = jnp.sum(left_scale[:, :, None, None] * wide[:, 0], axis=0)
-    enter_right = jnp.sum(right_scale[:, :, None, None] * wide[:, 1], axis=0)
+    scale = jnp.concatenate([left_scale, right_scale], axis=1)
+    scale = jnp.repeat(scale, cut // (2 * heads), axis=1)[:, :, None]
+    entering = jnp.sum(scale * arrived[:, :cut].astype(jnp.float32), axis=0)
+    enter_left, enter_right = entering.reshape(2, heads, width, width)
     total_left = jnp.exp(jnp.sum(jnp.where((place < me)[:, None], logs, 0.0), axis=0))
     total_right = jnp.exp(jnp.sum(jnp.where((place > me)[:, None], logs, 0.0), axis=0))
     return (total_left, enter_left), (total_right, enter_right)

time: 261 us -> 250 us (0.958)
  other arithmetic: 29.5 us -> 23.8 us
  local copies, waits for them, and re-layouts: 12.9 us -> 8.95 us
    convert_element_type x1 -> x0, local copies, waits for them, and re-layouts: 6.96 us -> none  [fast_prefix(): wide = states.astype(jnp.float32)]
    convert_element_type x1 -> x0, other arithmetic: 4.01 us -> none  [fast_prefix(): wide = states.astype(jnp.float32)]
  transfers between devices with their start and end apart: 3 -> 3, of which waited for: 1 -> 1; matrix products, arithmetic and copies ran while one was open for 10% -> 6% of each run, Pallas kernels for 20% -> 21%
where the time goes in v1:
time: 250 us
  Pallas kernels  199 us (80%)
  other arithmetic  23.8 us (10%)
  local copies, waits for them, and re-layouts  8.95 us (4%)
  matrix products  5.85 us (2%)
  starting transfers between devices  5.7 us (2%)
  waiting for transfers between devices  3.59 us (1%)
  blocking collectives  2.5 us (1%)
    pallas_call x1, Pallas kernels, project(): pl.pallas_call(functools.partial(project_kernel, count), out_shape=(jax.S...  148 us
    pallas_call x1, Pallas kernels, gather_small(): pl.pallas_call(functools.partial(gather_kernel, count), out_shape=jax.Sha...  26.1 us
    pallas_call x1, Pallas kernels, fast_retention(): pl.pallas_call(retain_kernel, grid=(blocks,), in_specs=[pl.BlockSpec((len...  15.3 us
    pallas_call x1, Pallas kernels, fast_states(): pl.pallas_call(states_kernel, grid=(blocks,), in_specs=[rows, scale, scal...  9.85 us
    reduce_sum x1, other arithmetic, body(): jnp.sum(convolved, axis=1)  6.77 us
    dot_general x1, matrix products, body(): jnp.dot(jnp.concatenate([branch_out, heads_out], axis=1), out_weights, pr...  5.85 us
  transfers between devices with their start and end apart: 3, of which 1 were waited for; matrix products, arithmetic and copies ran while one was open for 6% of the time, Pallas kernels for 21%

profile of v1, /device:TPU:0, one launch (start us, length us, event | category | flops | bytes accessed | tf_op | source)
XLA Modules:
  0.0 249.7 jit_solution(2043739481244043047)
XLA Ops:
  0.0 1.3 stack_reshape.16
  1.4 1.4 stack_reshape.17
  2.8 0.6 pad_maximum_fusion.3
  3.6 0.2 copy.33
  4.0 1.1 pad_maximum_fusion.local
  5.1 147.6 %project.1 = (bf16[768,512]{1,0:T(8,128)(2,1)}, bf16[768,2048]{1,0:T(8,128)(2,1)}, bf16[1024,2048]{1,0:T(8,128)(2,1)}) custom-call(bf16[384,2048]{1,0:T(8,128)(2,1)} %tokens.1, f32[1,2048]{1,0:T(1,128)} %bitcast.107, bf16[4,128,1024]{2,1,0:T(8,128)(2,1)} %pad_maximum_fusion.local), custom_call_target="tpu_custom_call" | custom-call | tf_op jit(solution)/shard_map/project/pallas_call | solution.py:259
  152.8 0.7 fusion.50
  153.5 4.1 %collective-permute-start = (bf16[15,512]{1,0:T(8,128)(2,1)S(1)}, bf16[15,512]{1,0:T(8,128)(2,1)S(1)}, u32[]{:S(2)}, u32[]{:S(2)}) collective-permute-start(bf16[15,512]{1,0:T(8,128)(2,1)S(1)} %get-tuple-element.45), channel_id=1, source_target_pairs={{0,2},{2,4},{4,6},{6,8},{8,10},{10,12},{12,14},{14,16},{16,18},{18... | collective-permute-start | bytes 46088 | tf_op jit(solution)/shard_map/ppermute | solution.py:327
  157.6 1.5 collective-permute-start.1
  159.2 1.7 reduce-window.6
  161.2 0.2 slice_reduce_fusion.2
  161.5 1.0 copy.28.end_scale
  162.4 0.9 copy.29.start_scale
  163.4 9.9 %block_states.1 = (f32[3,8,64,64]{3,2,1,0:T(8,128)}, f32[3,8,64,64]{3,2,1,0:T(8,128)}) custom-call(bf16[768,2048]{1,0:T(8,128)(2,1)} %get-tuple-element.23.packed, f32[768,8]{1,0:T(8,128)} %copy.28.end_scale, f32[768,8]{1,0:T(8,128)} %copy.29.start_scale), custom_call_target="tpu_custom_call" | custom-call | tf_op jit(solution)/shard_map/block_states/pallas_call | solution.py:435
  173.2 1.5 add_convert_fusion.1
  175.1 0.7 maximum_bitcast_fusion.2.local
  175.8 26.1 %gather_states.1 = bf16[1,16,528,128]{3,2,1,0:T(8,128)(2,1)} custom-call(bf16[1,528,128]{2,1,0:T(8,128)(2,1)} %maximum_bitcast_fusion.2.local), custom_call_target="tpu_custom_call" | custom-call | tf_op jit(solution)/shard_map/gather_states/pallas_call | solution.py:301
  201.8 0.8 slice_convert_fusion
  203.4 3.3 %multiply_reduce_fusion = f32[512,128]{1,0:T(8,128)S(1)} fusion(bf16[16,528,128]{2,1,0:T(8,128)(2,1)} %bitcast.95, f32[16,512]{1,0:T(8,128)S(1)} %mul.589), kind=kLoop, calls=%fused_computation | loop fusion | flops 3080192 | bytes 2392064 | tf_op jit(solution)/shard_map/reduce_sum | solution.py:556
  207.0 0.2 multiply_add_fusion.1
  207.3 1.0 pad_maximum_fusion.2.backward_in
  208.4 1.0 pad_maximum_fusion.1.forward_in
  209.4 0.9 copy.31.column
  210.3 15.3 %retain.1 = bf16[768,512]{1,0:T(8,128)(2,1)} custom-call(bf16[768,2048]{1,0:T(8,128)(2,1)} %get-tuple-element.23.packed, f32[768,8]{1,0:T(8,128)} %copy.31.column, f32[3,8,256]{2,1,0:T(8,128)} %bitcast.102, f32[3,8,64,64]{3,2,1,0:T(8,128)} %pad_maximum_fusion.1.forward_in, f32[3,8,64,64]{3,2,1,0:T(8,128)} %pad_maximum_fusion.2.backward_in, f32[1,512]{1,0:T(1,128)} %bitcast.139), custom_call_target="tpu_custom_call" | custom-call | tf_op jit(solution)/shard_map/retain/pallas_call | solution.py:489
  225.6 0.2 maximum_convert_fusion
  225.9 6.8 %fusion.48 = (f32[768]{0:T(1024)S(1)}, f32[768]{0:T(1024)S(1)}, f32[768,512]{1,0:T(8,128)S(1)}) fusion(f32[798,512]{1,0:T(8,128)S(1)} %maximum_convert_fusion, f32[512]{0:T(512)S(1)} %bitcast.137, f32[512]{0:T(512)S(1)} %bitcast.138, f32[512]{0:T(512)S(1)} %bitcast.109, f32[512]{0:T(512)S(1)} %bitcast.110, f32[512]{0:T(512)S(1)} %bitcast.111, ...), kind=kLoop, calls=%fused_computation.138 | loop fusion | flops 25164288 | bytes 50401280 | tf_op jit(solution)/shard_map/reduce_sum | solution.py:619
  232.7 2.5 %all-reduce.1 = (f32[768]{0:T(1024)S(1)}, f32[768]{0:T(1024)S(1)}) all-reduce(f32[768]{0:T(1024)S(1)} %get-tuple-element.28, f32[768]{0:T(1024)S(1)} %get-tuple-element.27), channel_id=1, replica_groups=mesh['sp'=16,'tp'=2] {'tp'}, use_global_device_ids=true, to_apply=%region_3.0 | all-reduce | flops 1536 | bytes 12288 | tf_op jit(solution)/shard_map/psum | solution.py:619
  235.2 0.5 multiply_convert_fusion
  235.7 5.8 %convolution_convert_fusion = bf16[768,2048]{1,0:T(8,128)(2,1)S(1)} fusion(bf16[1024,2048]{1,0:T(8,128)(2,1)} %get-tuple-element.26, bf16[768,512]{1,0:T(8,128)(2,1)} %retain.1, bf16[768,512]{1,0:T(8,128)(2,1)S(1)} %multiply_convert_fusion), kind=kOutput, calls=%fused_computation.1 | convolution fusion | flops 3225944064 | bytes 8912896 | tf_op jit(solution)/shard_map/dot_general | solution.py:687
  241.6 1.3 dynamic-slice_bitcast_fusion
  243.0 3.6 %collective-permute-done.2 = bf16[384,2048]{1,0:T(8,128)(2,1)} collective-permute-done((bf16[384,2048]{1,0:T(8,128)(2,1)}, bf16[384,2048]{1,0:T(8,128)(2,1)}, u32[]{:S(2)}, u32[]{:S(2)}) %collective-permute-start.2) | collective-permute-done | bytes 1572896 | tf_op jit(solution)/shard_map/ppermute | solution.py:696
  246.6 3.2 %fusion = bf16[384,2048]{1,0:T(8,128)(2,1)} fusion(bf16[384,2048]{1,0:T(8,128)(2,1)} %collective-permute-done.2, bf16[2,384,2048]{2,1,0:T(8,128)(2,1)S(1)} %bitcast.97, s32[]{:T(128)S(6)} %select_n.33), kind=kLoop, calls=%fused_computation.3 | loop fusion | flops 3145728 | bytes 4718596 | tf_op jit(solution)/shard_map/convert_element_type | solution.py:697
  (68 shorter events, 2.5 us)
Async XLA Ops:
  0.0 3.6 %copy-start.6 = (bf16[512,128]{1,0:T(8,128)(2,1)S(1)}, bf16[512,128]{1,0:T(8,128)(2,1)}, u32[]{:S(2)}) copy-start(bf16[512,128]{1,0:T(8,128)(2,1)} %param.30) | copy-start | bytes 393220
  0.0 3.6 %copy-start.5 = (bf16[512,128]{1,0:T(8,128)(2,1)S(1)}, bf16[512,128]{1,0:T(8,128)(2,1)}, u32[]{:S(2)}) copy-start(bf16[512,128]{1,0:T(8,128)(2,1)} %param.31) | copy-start | bytes 393220
  1.4 2.6 %copy-start.7 = (bf16[128,512]{1,0:T(8,128)(2,1)S(1)}, bf16[128,512]{1,0:T(8,128)(2,1)}, u32[]{:S(2)}) copy-start(bf16[128,512]{1,0:T(8,128)(2,1)} %param.22) | copy-start | bytes 393220
  1.4 2.6 %copy-start.8 = (bf16[128,512]{1,0:T(8,128)(2,1)S(1)}, bf16[128,512]{1,0:T(8,128)(2,1)}, u32[]{:S(2)}) copy-start(bf16[128,512]{1,0:T(8,128)(2,1)} %param.21) | copy-start | bytes 393220
  1.4 2.6 %copy-start.9 = (bf16[128,512]{1,0:T(8,128)(2,1)S(1)}, bf16[128,512]{1,0:T(8,128)(2,1)}, u32[]{:S(2)}) copy-start(bf16[128,512]{1,0:T(8,128)(2,1)} %param.24) | copy-start | bytes 393220
  1.4 2.6 %copy-start.10 = (bf16[128,512]{1,0:T(8,128)(2,1)S(1)}, bf16[128,512]{1,0:T(8,128)(2,1)}, u32[]{:S(2)}) copy-start(bf16[128,512]{1,0:T(8,128)(2,1)} %param.23) | copy-start | bytes 393220
  5.1 153.9 %copy-start.11 = (f32[31,512]{1,0:T(8,128)S(1)}, f32[31,512]{1,0:T(8,128)}, u32[]{:S(2)}) copy-start(f32[31,512]{1,0:T(8,128)} %param.25) | copy-start | bytes 190468
  5.1 154.0 %copy-start.12 = (f32[8,768]{1,0:T(8,128)S(1)}, f32[8,768]{1,0:T(8,128)}, u32[]{:S(2)}) copy-start(f32[8,768]{1,0:T(8,128)} %param.27) | copy-start | bytes 73732
  153.5 72.1 %collective-permute-start = (bf16[15,512]{1,0:T(8,128)(2,1)S(1)}, bf16[15,512]{1,0:T(8,128)(2,1)S(1)}, u32[]{:S(2)}, u32[]{:S(2)}) collective-permute-start(bf16[15,512]{1,0:T(8,128)(2,1)S(1)} %get-tuple-element.45), channel_id=1, source_target_pairs={{0,2},{2,4},{4,6},{6,8},{8,10},{10,12},{12,14},{14,16},{16,18},{18... | collective-permute-start | bytes 46088 | tf_op jit(solution)/shard_map/ppermute | solution.py:327
  157.6 68.0 %collective-permute-start.1 = (bf16[15,512]{1,0:T(8,128)(2,1)S(1)}, bf16[15,512]{1,0:T(8,128)(2,1)S(1)}, u32[]{:S(2)}, u32[]{:S(2)}) collective-permute-start(bf16[15,512]{1,0:T(8,128)(2,1)S(1)} %get-tuple-element.46), channel_id=1, source_target_pairs={{2,0},{4,2},{6,4},{8,6},{10,8},{12,10},{14,12},{16,14},{18,16},{20... | collective-permute-start | bytes 46088 | tf_op jit(solution)/shard_map/ppermute | solution.py:328
  161.2 48.2 %copy-start.4 = (f32[3,8,2,128]{3,1,2,0:T(8,128)}, f32[3,8,2,128]{3,1,2,0:T(8,128)S(1)}, u32[]{:S(2)}) copy-start(f32[3,8,2,128]{3,1,2,0:T(8,128)S(1)} %get-tuple-element.44) | copy-start | bytes 73732
  203.4 3.6 %copy-start = (f32[3,8,64,64]{3,2,1,0:T(8,128)S(1)}, f32[3,8,64,64]{3,2,1,0:T(8,128)}, u32[]{:S(2)}) copy-start(f32[3,8,64,64]{3,2,1,0:T(8,128)} %get-tuple-element.25) | copy-start | bytes 1179652
  203.4 3.6 %copy-start.1 = (f32[3,8,64,64]{3,2,1,0:T(8,128)S(1)}, f32[3,8,64,64]{3,2,1,0:T(8,128)}, u32[]{:S(2)}) copy-start(f32[3,8,64,64]{3,2,1,0:T(8,128)} %get-tuple-element.24) | copy-start | bytes 1179652
  203.4 3.6 %copy-start.3 = (f32[2,8,64,64]{3,2,1,0:T(8,128)S(1)}, f32[2,8,64,64]{3,2,1,0:T(8,128)}, u32[]{:S(2)}) copy-start(f32[2,8,64,64]{3,2,1,0:T(8,128)} %param.28) | copy-start | bytes 786436
  210.3 15.3 %copy-start.2 = (bf16[768,512]{1,0:T(8,128)(2,1)S(1)}, bf16[768,512]{1,0:T(8,128)(2,1)}, u32[]{:S(2)}) copy-start(bf16[768,512]{1,0:T(8,128)(2,1)} %get-tuple-element.22) | copy-start | bytes 2359300
  225.9 9.3 %copy-start.13 = (f32[512]{0:T(512)S(1)}, f32[512]{0:T(512)}, u32[]{:S(2)}) copy-start(f32[512]{0:T(512)} %param.26) | copy-start | bytes 6148
  242.8 3.8 %collective-permute-start.2 = (bf16[384,2048]{1,0:T(8,128)(2,1)}, bf16[384,2048]{1,0:T(8,128)(2,1)}, u32[]{:S(2)}, u32[]{:S(2)}) collective-permute-start(bf16[384,2048]{1,0:T(8,128)(2,1)} %dynamic-slice_bitcast_fusion), channel_id=1, source_target_pairs={{0,1},{1,0},{2,3},{3,2},{4,5},{5,4},{6,7},{7,6},{8,9},{9,8},{10,11... | collective-permute-start | bytes 4718600 | tf_op jit(solution)/shard_map/ppermute | solution.py:696
